TPU v7x, 32 devices: a whole 2x2x4 slice. The times are simulated.
32 devices in a mesh: tp: 8 (over z, y), dp: 4 (over x, core).
Axes of the slice: x: 2, y: 2, z: 4, core: 2. Of those that a mesh axis runs over, the one named last changes fastest.
Arguments:
- stream: bfloat16 [256, 2048], P('tp', 'dp'), may hold values from -12 to 12
- norm_gain: float32 [2, 2048], P(None, 'dp'), may hold values from 0.1 to 1.9
- w_input: bfloat16 [2, 2048, 2048], P(None, 'dp', 'tp'), may hold values from -0.125 to 0.125
- lam_re: float32 [2, 128, 64], P(None, 'tp'), may hold values from -1 to -0.05
- lam_im: float32 [2, 128, 64], P(None, 'tp'), may hold values from 0 to 6
- log_dt: float32 [2, 128], P(None, 'tp'), may hold values from -3 to 0
- b_re: float32 [2, 128, 64, 16], P(None, 'tp'), may hold values from -1 to 1
- b_im: float32 [2, 128, 64, 16], P(None, 'tp'), may hold values from -1 to 1
- readout_real: float32 [2, 128, 16, 64], P(None, 'tp'), may hold values from -0.5 to 0.5
- readout_imaginary: float32 [2, 128, 16, 64], P(None, 'tp'), may hold values from -0.5 to 0.5
- d_skip: float32 [2, 2048], P(None, 'tp'), may hold values from -4 to 4
- w_val: bfloat16 [2, 2048, 2048], P(None, 'tp', 'dp'), may hold values from -0.375 to 0.375
- w_gate: bfloat16 [2, 2048, 2048], P(None, 'tp', 'dp'), may hold values from -0.375 to 0.375
- state: float32 [2, 256, 128, 128], P(None, 'dp', 'tp'), may hold values from -6 to 6
Outputs:
- stream_out: bfloat16 [256, 2048], P('tp', 'dp')
- states_out: float32 [2, 256, 128, 128], P(None, 'dp', 'tp')
All inputs are finite; a program needn't handle non-finite values.
Results may differ from a plain program's by a relative error of at most 0.0064.
Values may be sent and summed in bfloat16 or wider, within the bound.
A program may use at most 64 MiB of HBM per device.

v0:
```python
import jax
import jax.numpy as jnp
from jax import lax
from jax.sharding import PartitionSpec as P

D = 2048
LAYERS = 2
eps = 1e-06


def advance(
    inputs, old_state, lam_re, lam_im, log_dt, b_re, b_im, readout_real, readout_imaginary, d_skip
):
    upper_bound = lax.Precision.HIGHEST
    count_rows, groups, doubled = old_state.shape
    half_state = doubled // 2
    chans = b_re.shape[-1]
    step_size = jnp.exp(log_dt)[:, None]
    decay = jnp.exp(lam_re * step_size)
    angle = lam_im * step_size
    keep_re = decay * jnp.cos(angle)
    keep_im = decay * jnp.sin(angle)
    denom = lam_re * lam_re + lam_im * lam_im
    ratio_re = ((keep_re - 1.0) * lam_re + keep_im * lam_im) / denom
    ratio_im = (keep_im * lam_re - (keep_re - 1.0) * lam_im) / denom
    drive_re = ratio_re[..., None] * b_re - ratio_im[..., None] * b_im
    drive_im = ratio_re[..., None] * b_im + ratio_im[..., None] * b_re
    grouped = inputs.reshape(count_rows, groups, chans)
    push_re = jnp.einsum("gpc,rgc->rgp", drive_re, grouped, precision=upper_bound)
    push_im = jnp.einsum("gpc,rgc->rgp", drive_im, grouped, precision=upper_bound)
    old_re = old_state[..., :half_state]
    old_im = old_state[..., half_state:]
    updated_real = keep_re * old_re - keep_im * old_im + push_re
    updated_imaginary = keep_re * old_im + keep_im * old_re + push_im
    readout_output = jnp.einsum(
        "aot,mat->mao", readout_real, updated_real, precision=upper_bound
    ) - jnp.einsum("aot,mat->mao", readout_imaginary, updated_imaginary, precision=upper_bound)
    pre_act = readout_output.reshape(count_rows, groups * chans) + d_skip * inputs
    return (pre_act, jnp.concatenate([updated_real, updated_imaginary], axis=-1))


def half_output(mixed_all, val_part, gate_part):
    return jnp.concatenate(
        [
            jnp.dot(mixed_all, val_part, preferred_element_type=jnp.float32),
            jnp.dot(mixed_all, gate_part, preferred_element_type=jnp.float32),
        ],
        axis=1,
    )


def per_device(
    stream,
    norm_gain,
    w_input,
    lam_re,
    lam_im,
    log_dt,
    b_re,
    b_im,
    readout_real,
    readout_imaginary,
    d_skip,
    w_val,
    w_gate,
    state,
):
    collected = []
    for layer_no in range(LAYERS):
        gathered = lax.all_gather(stream, "tp", axis=0, tiled=True)
        widened = gathered.astype(jnp.float32)
        normed = (widened * norm_gain[layer_no]).astype(jnp.bfloat16)
        square_part = jnp.sum(widened * widened, axis=1)
        weight_in = w_input[layer_no]
        partial_value = jnp.dot(normed, weight_in, preferred_element_type=jnp.float32)
        summed, square_total = (
            lax.psum_scatter(partial_value, "dp", scatter_dimension=0, tiled=True),
            lax.psum_scatter(square_part, "dp", scatter_dimension=0, tiled=True),
        )
        inputs = lax.rsqrt(square_total / D + eps)[:, None] * summed
        pre_act, new_state = advance(
            inputs,
            state[layer_no],
            lam_re[layer_no],
            lam_im[layer_no],
            log_dt[layer_no],
            b_re[layer_no],
            b_im[layer_no],
            readout_real[layer_no],
            readout_imaginary[layer_no],
            d_skip[layer_no],
        )
        mixed = jax.nn.gelu(pre_act).astype(jnp.bfloat16)
        mixed_all = lax.all_gather(mixed, "dp", axis=0, tiled=True)
        columns = w_val.shape[2]
        combined = lax.psum_scatter(
            half_output(mixed_all, w_val[layer_no], w_gate[layer_no]),
            "tp",
            scatter_dimension=0,
            tiled=True,
        )
        value = combined[:, :columns]
        gate = combined[:, columns:]
        stream = (stream.astype(jnp.float32) + value * jax.nn.sigmoid(gate)).astype(jnp.bfloat16)
        collected.append(new_state)
    return (stream, jnp.stack(collected))


def solution(mesh):
    return jax.shard_map(
        per_device,
        mesh=mesh,
        in_specs=(
            P("tp", "dp"),
            P(None, "dp"),
            P(None, "dp", "tp"),
            P(None, "tp", None),
            P(None, "tp", None),
            P(None, "tp"),
            P(None, "tp", None, None),
            P(None, "tp", None, None),
            P(None, "tp", None, None),
            P(None, "tp", None, None),
            P(None, "tp"),
            P(None, "tp", "dp"),
            P(None, "tp", "dp"),
            P(None, "dp", "tp", None),
        ),
        out_specs=(P("tp", "dp"), P(None, "dp", "tp", None)),
        check_vma=False,
    )
```

profile of v0, /device:TPU:0, one launch (start us, length us, event | category | flops | bytes accessed | tf_op | source)
XLA Modules:
  0.0 278.8 jit_solution(17151186009216203104)
XLA Ops:
  7.2 0.8 fusion.109
  8.0 32.8 %all_gather.12 = bf16[256,512]{1,0:T(8,128)(2,1)S(1)} all-gather(bf16[32,512]{1,0:T(8,128)(2,1)} %param.14), channel_id=1, replica_groups=mesh['tp'=8,'dp'=4] {'tp'}, dimensions={0}, use_global_device_ids=true | all-gather | bytes 294912 | tf_op jit(solution)/shard_map/all_gather | solution.py:70
  40.8 1.9 fusion.10
  42.8 0.7 copy-done.18
  43.4 0.1 multiply_bitcast_fusion.1
  43.6 0.2 fusion.93
  43.8 0.1 fusion.4
  43.9 0.5 copy-done.17
  44.4 5.6 %all-reduce = f32[256]{0:T(256)S(1)} all-reduce(f32[256]{0:T(256)S(1)} %fusion.4), channel_id=2, replica_groups=mesh['tp'=8,'dp'=4] {'dp'}, use_global_device_ids=true, to_apply=%region_1.0.clone | all-reduce | flops 256 | bytes 2048
  50.1 0.7 copy-done.19
  50.7 0.6 dynamic-slice
  52.1 0.3 copy_bitcast_fusion
  52.5 11.4 %reduce-scatter.5.cloned.1.call-done = f32[64,256]{1,0:T(8,128)} async-done(((f32[256,256]{1,0:T(8,128)}), f32[64,256]{1,0:T(8,128)}) %reduce-scatter.5.cloned.1.call-update) | async-done | bytes 65552 | tf_op jit(solution)/shard_map/reduce_scatter | solution.py:77
  63.9 0.9 broadcast_multiply_fusion.1
  64.9 1.0 fusion.3
  65.9 1.0 fusion.2
  67.0 0.9 fusion.38
  68.0 0.9 convolution_subtract_fusion.1
  69.0 0.8 copy-done.10
  69.7 0.1 fusion.63
  69.8 5.5 %all_gather.13 = bf16[256,256]{1,0:T(8,128)(2,1)S(1)} all-gather(bf16[64,256]{1,0:T(8,128)(2,1)S(1)} %fusion.63), channel_id=1, replica_groups=mesh['tp'=8,'dp'=4] {'dp'}, dimensions={0}, use_global_device_ids=true | all-gather | bytes 163840 | tf_op jit(solution)/shard_map/all_gather | solution.py:94
  75.4 0.2 fusion.17
  75.6 0.2 fusion.19
  75.9 1.1 pad_maximum_fusion
  77.0 64.3 %reduce-scatter.7.cloned.1.call-done = f32[32,1024]{1,0:T(8,128)} async-done(((f32[256,1024]{1,0:T(8,128)}), f32[32,1024]{1,0:T(8,128)}) %reduce-scatter.7.cloned.1.call-update) | async-done | bytes 131088 | tf_op jit(solution)/shard_map/reduce_scatter | solution.py:96
  141.4 0.9 fusion.90
  142.3 30.9 %all_gather.14 = bf16[256,512]{1,0:T(8,128)(2,1)S(1)} all-gather(bf16[32,512]{1,0:T(8,128)(2,1)S(1)} %fusion.90), channel_id=1, replica_groups=mesh['tp'=8,'dp'=4] {'tp'}, dimensions={0}, use_global_device_ids=true | all-gather | bytes 294912 | tf_op jit(solution)/shard_map/all_gather | solution.py:70
  173.1 0.9 fusion.8
  174.1 0.1 fusion.6
  174.3 5.7 %all-reduce.1 = f32[256]{0:T(256)S(1)} all-reduce(f32[256]{0:T(256)S(1)} %fusion.6), channel_id=5, replica_groups=mesh['tp'=8,'dp'=4] {'dp'}, use_global_device_ids=true, to_apply=%region_5.0.clone | all-reduce | flops 256 | bytes 2048
  180.0 13.2 %reduce-scatter.9.cloned.1.call-done = f32[64,256]{1,0:T(8,128)} async-done(((f32[256,256]{1,0:T(8,128)}), f32[64,256]{1,0:T(8,128)}) %reduce-scatter.9.cloned.1.call-update) | async-done | bytes 65552 | tf_op jit(solution)/shard_map/reduce_scatter | solution.py:77
  193.2 0.9 broadcast_multiply_fusion
  194.3 1.0 fusion
  195.3 1.0 fusion.1
  196.4 0.9 fusion.31
  197.3 0.9 convolution_subtract_fusion
  198.4 0.8 copy-done.11
  199.1 0.1 fusion.71
  199.2 5.5 %all_gather.15 = bf16[256,256]{1,0:T(8,128)(2,1)S(1)} all-gather(bf16[64,256]{1,0:T(8,128)(2,1)S(1)} %fusion.71), channel_id=1, replica_groups=mesh['tp'=8,'dp'=4] {'dp'}, dimensions={0}, use_global_device_ids=true | all-gather | bytes 163840 | tf_op jit(solution)/shard_map/all_gather | solution.py:94
  204.8 0.2 fusion.12
  205.0 0.2 fusion.14
  205.2 1.1 pad_maximum_fusion.1
  206.3 0.2 maximum_bitcast_fusion
  206.5 0.2 maximum_bitcast_fusion.1
  206.8 0.1 pad_maximum_fusion.2
  206.9 1.6 copy.38
  208.5 62.3 %reduce-scatter.11.cloned.1.call-done = f32[32,1024]{1,0:T(8,128)} async-done(((f32[256,1024]{1,0:T(8,128)}), f32[32,1024]{1,0:T(8,128)}) %reduce-scatter.11.cloned.1.call-update) | async-done | bytes 131088 | tf_op jit(solution)/shard_map/reduce_scatter | solution.py:96
  270.7 1.5 fusion.91
  (52 shorter events, 0.9 us)
Async XLA Ops:
  7.2 44.9 %copy-start.2 = (f32[2,64,16,128]{3,2,1,0:T(8,128)S(1)}, f32[2,64,16,128]{3,2,1,0:T(8,128)}, u32[]{:S(2)}) copy-start(f32[2,64,16,128]{3,2,1,0:T(8,128)} %param.27) | copy-start | bytes 3145732
  7.2 56.7 %reduce-scatter.5.cloned.1.call-start = ((), (), s32[]{:S(2)}) async-start(), calls=%async_computation.4 | async-start | bytes 327680 | tf_op jit(solution)/shard_map/reduce_scatter | solution.py:77
  42.7 0.8 copy-start.15
  42.7 0.8 copy-start.16
  42.7 98.7 %reduce-scatter.7.cloned.1.call-start = ((), (), s32[]{:S(2)}) async-start(), calls=%async_computation.5 | async-start | bytes 1179648 | tf_op jit(solution)/shard_map/reduce_scatter | solution.py:96
  42.7 0.7 copy-start.18
  43.7 0.7 copy-start.17
  50.1 0.7 copy-start.19
  52.1 12.7 %copy-start.1 = (f32[2,16,64,16]{2,3,1,0:T(8,128)S(1)}, f32[2,16,64,16]{2,3,1,0:T(8,128)}, u32[]{:S(2)}) copy-start(f32[2,16,64,16]{2,3,1,0:T(8,128)} %param.20) | copy-start | bytes 393220
  52.5 12.4 %copy-start = (f32[2,16,64,16]{2,3,1,0:T(8,128)S(1)}, f32[2,16,64,16]{2,3,1,0:T(8,128)}, u32[]{:S(2)}) copy-start(f32[2,16,64,16]{2,3,1,0:T(8,128)} %param.21) | copy-start | bytes 393220
  65.9 1.1 copy-start.12
  67.0 1.0 copy-start.8
  68.0 7.5 %copy-start.4 = (bf16[2,256,512]{2,1,0:T(8,128)(2,1)S(1)}, bf16[2,256,512]{2,1,0:T(8,128)(2,1)}, u32[]{:S(2)}) copy-start(bf16[2,256,512]{2,1,0:T(8,128)(2,1)} %param.26) | copy-start | bytes 1572868
  68.9 0.9 copy-start.10
  69.8 5.8 %copy-start.6 = (bf16[2,256,512]{2,1,0:T(8,128)(2,1)S(1)}, bf16[2,256,512]{2,1,0:T(8,128)(2,1)}, u32[]{:S(2)}) copy-start(bf16[2,256,512]{2,1,0:T(8,128)(2,1)} %param.25) | copy-start | bytes 1572868
  76.9 64.4 %copy-start.14 = (bf16[32,512]{1,0:T(8,128)(2,1)S(1)}, bf16[32,512]{1,0:T(8,128)(2,1)}, u32[]{:S(2)}) copy-start(bf16[32,512]{1,0:T(8,128)(2,1)} %param.14) | copy-start | bytes 98308
  76.9 96.2 %copy-start.3 = (bf16[2,512,256]{2,1,0:T(8,128)(2,1)S(1)}, bf16[2,512,256]{2,1,0:T(8,128)(2,1)}, u32[]{:S(2)}) copy-start(bf16[2,512,256]{2,1,0:T(8,128)(2,1)} %param.16) | copy-start | bytes 1572868
  77.0 116.3 %reduce-scatter.9.cloned.1.call-start = ((), (), s32[]{:S(2)}) async-start(), calls=%async_computation.6 | async-start | bytes 327680 | tf_op jit(solution)/shard_map/reduce_scatter | solution.py:77
  174.1 96.6 %reduce-scatter.11.cloned.1.call-start = ((), (), s32[]{:S(2)}) async-start(), calls=%async_computation.7 | async-start | bytes 1179648 | tf_op jit(solution)/shard_map/reduce_scatter | solution.py:96
  195.3 1.1 copy-start.13
  196.4 1.0 copy-start.9
  197.3 7.4 %copy-start.5 = (bf16[2,256,512]{2,1,0:T(8,128)(2,1)S(1)}, bf16[2,256,512]{2,1,0:T(8,128)(2,1)}, u32[]{:S(2)}) copy-start(bf16[2,256,512]{2,1,0:T(8,128)(2,1)} %param.26) | copy-start | bytes 1572868
  198.3 0.9 copy-start.11
  199.2 5.8 %copy-start.7 = (bf16[2,256,512]{2,1,0:T(8,128)(2,1)S(1)}, bf16[2,256,512]{2,1,0:T(8,128)(2,1)}, u32[]{:S(2)}) copy-start(bf16[2,256,512]{2,1,0:T(8,128)(2,1)} %param.25) | copy-start | bytes 1572868
Sparse Core Ops, SparseCore 0:
  42.8 21.0 reduce-scatter.4
  77.1 64.2 reduce-scatter.6
  174.2 18.9 reduce-scatter.8
  206.5 64.2 reduce-scatter.10
where the time goes:
time: 279 us
  waiting for transfers between devices  151 us (54%)
  blocking collectives  86 us (31%)
  between operations  14.7 us (5%)
  matrix products  11.6 us (4%)
  other arithmetic  7.83 us (3%)
  local copies, waits for them, and re-layouts  7.2 us (3%)
    reduce_scatter x2, waiting for transfers between devices, per_device(): lax.psum_scatter(half_output(mixed_all, w_val[layer_no], w_gate[layer_no]...  127 us
    all_gather x2, blocking collectives, per_device(): gathered = lax.all_gather(stream, 'tp', axis=0, tiled=True)  63.6 us
    reduce_scatter x2, waiting for transfers between devices, per_device(): lax.psum_scatter(partial_value, 'dp', scatter_dimension=0, tiled=True)  24.6 us
    unnamed x2, blocking collectives  11.3 us
    all_gather x2, blocking collectives, per_device(): mixed_all = lax.all_gather(mixed, 'dp', axis=0, tiled=True)  11.1 us
    unnamed x42, local copies, waits for them, and re-layouts  5.66 us
  transfers between devices with their start and end apart: 4, of which 4 were waited for; matrix products, arithmetic and copies ran while one was open for 1% of the time, Pallas kernels for 0%

commit v1 on v0

--- a/solution.py
+++ b/solution.py
@@ -67,7 +67,16 @@
 ):
     collected = []
     for layer_no in range(LAYERS):
-        gathered = lax.all_gather(stream, "tp", axis=0, tiled=True)
+        lanes = lax.axis_size("tp")
+        t1 = sorted(((at, (at + 1) % lanes) for at in range(lanes)))
+        earlier = stream
+        chunks = [earlier]
+        for to_i in [*range(1, lanes)]:
+            earlier = lax.ppermute(earlier, "tp", t1)
+            chunks.insert(0, earlier)
+        vec_out = jnp.concatenate(chunks, 0)
+        block_out = lax.axis_index("tp") + 1
+        gathered = jnp.roll(vec_out, block_out * stream.shape[0], 0)
         widened = gathered.astype(jnp.float32)
         normed = (widened * norm_gain[layer_no]).astype(jnp.bfloat16)
         square_part = jnp.sum(widened * widened, axis=1)

time: 279 us -> 305 us (1.093)
  waiting for transfers between devices: 151 us -> 235 us
  blocking collectives: 86 us -> 22.4 us
  starting transfers between devices: 0.16 us -> 4.35 us
    ppermute x0 -> x14, waiting for transfers between devices: none -> 88.7 us  [per_device(): earlier = lax.ppermute(earlier, 'tp', t1)]
    all_gather x2 -> x0, blocking collectives: 63.6 us -> none  [per_device(): gathered = lax.all_gather(stream, 'tp', axis=0, tiled=True)]
    reduce_scatter x2, waiting for transfers between devices: 24.6 us -> 19.8 us  [per_device(): lax.psum_scatter(partial_value, 'dp', scatter_dimension=0, tiled=True)]
    ppermute x0 -> x14, starting transfers between devices: none -> 4.19 us  [per_device(): earlier = lax.ppermute(earlier, 'tp', t1)]
  transfers between devices with their start and end apart: 4 -> 18, of which waited for: 4 -> 18; matrix products, arithmetic and copies ran while one was open for 1% -> 2% of each run, Pallas kernels for 0% -> 0%
where the time goes in v1:
time: 305 us
  waiting for transfers between devices  235 us (77%)
  blocking collectives  22.4 us (7%)
  between operations  14.8 us (5%)
  matrix products  11.8 us (4%)
  other arithmetic  8.2 us (3%)
  local copies, waits for them, and re-layouts  7.87 us (3%)
  starting transfers between devices  4.35 us (1%)
    reduce_scatter x2, waiting for transfers between devices, per_device(): lax.psum_scatter(half_output(mixed_all, w_val[layer_no], w_gate[layer_no]...  127 us
    ppermute x14, waiting for transfers between devices, per_device(): earlier = lax.ppermute(earlier, 'tp', t1)  88.7 us
    reduce_scatter x2, waiting for transfers between devices, per_device(): lax.psum_scatter(partial_value, 'dp', scatter_dimension=0, tiled=True)  19.8 us
    unnamed x2, blocking collectives  11.3 us
    all_gather x2, blocking collectives, per_device(): mixed_all = lax.all_gather(mixed, 'dp', axis=0, tiled=True)  11.1 us
  transfers between devices with their start and end apart: 18, of which 18 were waited for; matrix products, arithmetic and copies ran while one was open for 2% of the time, Pallas kernels for 0%

profile of v1, /device:TPU:0, one launch (start us, length us, event | category | flops | bytes accessed | tf_op | source)
XLA Modules:
  0.0 304.8 jit_solution(7720905931886888201)
XLA Ops:
  7.2 3.0 collective-permute-start
  10.3 5.1 %collective-permute-done = bf16[32,512]{1,0:T(8,128)(2,1)S(1)} collective-permute-done((bf16[32,512]{1,0:T(8,128)(2,1)}, bf16[32,512]{1,0:T(8,128)(2,1)S(1)}, u32[]{:S(2)}, u32[]{:S(2)}) %collective-permute-start) | collective-permute-done | bytes 32800 | tf_op jit(solution)/shard_map/ppermute | solution.py:75
  15.4 6.6 %collective-permute-done.1 = bf16[32,512]{1,0:T(8,128)(2,1)S(1)} collective-permute-done((bf16[32,512]{1,0:T(8,128)(2,1)S(1)}, bf16[32,512]{1,0:T(8,128)(2,1)S(1)}, u32[]{:S(2)}, u32[]{:S(2)}) %collective-permute-start.1) | collective-permute-done | bytes 32800 | tf_op jit(solution)/shard_map/ppermute | solution.py:75
  22.0 1.3 fusion.112
  23.4 5.3 %collective-permute-done.2 = bf16[32,512]{1,0:T(8,128)(2,1)S(1)} collective-permute-done((bf16[32,512]{1,0:T(8,128)(2,1)S(1)}, bf16[32,512]{1,0:T(8,128)(2,1)S(1)}, u32[]{:S(2)}, u32[]{:S(2)}) %collective-permute-start.2) | collective-permute-done | bytes 32800 | tf_op jit(solution)/shard_map/ppermute | solution.py:75
  28.7 6.6 %collective-permute-done.3 = bf16[32,512]{1,0:T(8,128)(2,1)S(1)} collective-permute-done((bf16[32,512]{1,0:T(8,128)(2,1)S(1)}, bf16[32,512]{1,0:T(8,128)(2,1)S(1)}, u32[]{:S(2)}, u32[]{:S(2)}) %collective-permute-start.3) | collective-permute-done | bytes 32800 | tf_op jit(solution)/shard_map/ppermute | solution.py:75
  35.4 6.8 %collective-permute-done.4 = bf16[32,512]{1,0:T(8,128)(2,1)S(1)} collective-permute-done((bf16[32,512]{1,0:T(8,128)(2,1)S(1)}, bf16[32,512]{1,0:T(8,128)(2,1)S(1)}, u32[]{:S(2)}, u32[]{:S(2)}) %collective-permute-start.4) | collective-permute-done | bytes 32800 | tf_op jit(solution)/shard_map/ppermute | solution.py:75
  42.4 6.5 %collective-permute-done.5 = bf16[32,512]{1,0:T(8,128)(2,1)S(1)} collective-permute-done((bf16[32,512]{1,0:T(8,128)(2,1)S(1)}, bf16[32,512]{1,0:T(8,128)(2,1)S(1)}, u32[]{:S(2)}, u32[]{:S(2)}) %collective-permute-start.5) | collective-permute-done | bytes 32800 | tf_op jit(solution)/shard_map/ppermute | solution.py:75
  48.8 6.6 %collective-permute-done.6 = bf16[32,512]{1,0:T(8,128)(2,1)S(1)} collective-permute-done((bf16[32,512]{1,0:T(8,128)(2,1)S(1)}, bf16[32,512]{1,0:T(8,128)(2,1)S(1)}, u32[]{:S(2)}, u32[]{:S(2)}) %collective-permute-start.6) | collective-permute-done | bytes 32800 | tf_op jit(solution)/shard_map/ppermute | solution.py:75
  55.5 0.7 copy-done.12
  56.2 1.1 fusion.12
  57.4 0.6 copy-done.16
  58.0 0.7 copy-done.19
  58.7 0.6 dynamic-slice
  60.6 5.7 %all-reduce = f32[256]{0:T(256)S(1)} all-reduce(f32[256]{0:T(256)S(1)} %fusion.4), channel_id=2, replica_groups=mesh['tp'=8,'dp'=4] {'dp'}, use_global_device_ids=true, to_apply=%region_1.3.clone | all-reduce | flops 256 | bytes 2048
  66.3 8.5 %reduce-scatter.5.cloned.1.call-done = f32[64,256]{1,0:T(8,128)} async-done(((f32[256,256]{1,0:T(8,128)}), f32[64,256]{1,0:T(8,128)}) %reduce-scatter.5.cloned.1.call-update) | async-done | bytes 65552 | tf_op jit(solution)/shard_map/reduce_scatter | solution.py:86
  74.8 0.9 broadcast_multiply_fusion.1
  75.9 1.0 fusion.3
  76.9 1.0 fusion.2
  78.0 0.9 fusion.40
  78.9 0.9 convolution_subtract_fusion.1
  80.0 0.8 copy-done.8
  80.8 5.5 %all_gather.6 = bf16[256,256]{1,0:T(8,128)(2,1)S(1)} all-gather(bf16[64,256]{1,0:T(8,128)(2,1)S(1)} %fusion.65), channel_id=1, replica_groups=mesh['tp'=8,'dp'=4] {'dp'}, dimensions={0}, use_global_device_ids=true | all-gather | bytes 163840 | tf_op jit(solution)/shard_map/all_gather | solution.py:103
  86.8 1.1 pad_maximum_fusion
  88.0 64.4 %reduce-scatter.7.cloned.1.call-done = f32[32,1024]{1,0:T(8,128)} async-done(((f32[256,1024]{1,0:T(8,128)}), f32[32,1024]{1,0:T(8,128)}) %reduce-scatter.7.cloned.1.call-update) | async-done | bytes 131088 | tf_op jit(solution)/shard_map/reduce_scatter | solution.py:105
  152.4 0.9 fusion.92
  153.3 1.1 collective-permute-start.7
  154.4 5.6 %collective-permute-done.7 = bf16[32,512]{1,0:T(8,128)(2,1)S(1)} collective-permute-done((bf16[32,512]{1,0:T(8,128)(2,1)S(1)}, bf16[32,512]{1,0:T(8,128)(2,1)S(1)}, u32[]{:S(2)}, u32[]{:S(2)}) %collective-permute-start.7) | collective-permute-done | bytes 32800 | tf_op jit(solution)/shard_map/ppermute | solution.py:75
  159.9 6.6 %collective-permute-done.8 = bf16[32,512]{1,0:T(8,128)(2,1)S(1)} collective-permute-done((bf16[32,512]{1,0:T(8,128)(2,1)S(1)}, bf16[32,512]{1,0:T(8,128)(2,1)S(1)}, u32[]{:S(2)}, u32[]{:S(2)}) %collective-permute-start.8) | collective-permute-done | bytes 32800 | tf_op jit(solution)/shard_map/ppermute | solution.py:75
  166.5 6.7 %collective-permute-done.9 = bf16[32,512]{1,0:T(8,128)(2,1)S(1)} collective-permute-done((bf16[32,512]{1,0:T(8,128)(2,1)S(1)}, bf16[32,512]{1,0:T(8,128)(2,1)S(1)}, u32[]{:S(2)}, u32[]{:S(2)}) %collective-permute-start.9) | collective-permute-done | bytes 32800 | tf_op jit(solution)/shard_map/ppermute | solution.py:75
  173.3 6.6 %collective-permute-done.10 = bf16[32,512]{1,0:T(8,128)(2,1)S(1)} collective-permute-done((bf16[32,512]{1,0:T(8,128)(2,1)S(1)}, bf16[32,512]{1,0:T(8,128)(2,1)S(1)}, u32[]{:S(2)}, u32[]{:S(2)}) %collective-permute-start.10) | collective-permute-done | bytes 32800 | tf_op jit(solution)/shard_map/ppermute | solution.py:75
  179.9 6.6 %collective-permute-done.11 = bf16[32,512]{1,0:T(8,128)(2,1)S(1)} collective-permute-done((bf16[32,512]{1,0:T(8,128)(2,1)S(1)}, bf16[32,512]{1,0:T(8,128)(2,1)S(1)}, u32[]{:S(2)}, u32[]{:S(2)}) %collective-permute-start.11) | collective-permute-done | bytes 32800 | tf_op jit(solution)/shard_map/ppermute | solution.py:75
  186.5 6.6 %collective-permute-done.12 = bf16[32,512]{1,0:T(8,128)(2,1)S(1)} collective-permute-done((bf16[32,512]{1,0:T(8,128)(2,1)S(1)}, bf16[32,512]{1,0:T(8,128)(2,1)S(1)}, u32[]{:S(2)}, u32[]{:S(2)}) %collective-permute-start.12) | collective-permute-done | bytes 32800 | tf_op jit(solution)/shard_map/ppermute | solution.py:75
  193.1 6.6 %collective-permute-done.13 = bf16[32,512]{1,0:T(8,128)(2,1)S(1)} collective-permute-done((bf16[32,512]{1,0:T(8,128)(2,1)S(1)}, bf16[32,512]{1,0:T(8,128)(2,1)S(1)}, u32[]{:S(2)}, u32[]{:S(2)}) %collective-permute-start.13) | collective-permute-done | bytes 32800 | tf_op jit(solution)/shard_map/ppermute | solution.py:75
  199.8 2.0 fusion.10
  202.2 5.7 %all-reduce.1 = f32[256]{0:T(256)S(1)} all-reduce(f32[256]{0:T(256)S(1)} %fusion.6), channel_id=5, replica_groups=mesh['tp'=8,'dp'=4] {'dp'}, use_global_device_ids=true, to_apply=%region_5.7.clone | all-reduce | flops 256 | bytes 2048
  208.0 11.3 %reduce-scatter.9.cloned.1.call-done = f32[64,256]{1,0:T(8,128)} async-done(((f32[256,256]{1,0:T(8,128)}), f32[64,256]{1,0:T(8,128)}) %reduce-scatter.9.cloned.1.call-update) | async-done | bytes 65552 | tf_op jit(solution)/shard_map/reduce_scatter | solution.py:86
  219.3 0.9 broadcast_multiply_fusion
  220.3 1.0 fusion
  221.3 1.0 fusion.1
  222.4 0.9 fusion.33
  223.3 0.9 convolution_subtract_fusion
  224.4 0.8 copy-done.9
  225.2 5.5 %all_gather.7 = bf16[256,256]{1,0:T(8,128)(2,1)S(1)} all-gather(bf16[64,256]{1,0:T(8,128)(2,1)S(1)} %fusion.73), channel_id=1, replica_groups=mesh['tp'=8,'dp'=4] {'dp'}, dimensions={0}, use_global_device_ids=true | all-gather | bytes 163840 | tf_op jit(solution)/shard_map/all_gather | solution.py:103
  231.3 1.1 pad_maximum_fusion.1
  232.9 1.6 copy.38
  234.4 62.3 %reduce-scatter.11.cloned.1.call-done = f32[32,1024]{1,0:T(8,128)} async-done(((f32[256,1024]{1,0:T(8,128)}), f32[32,1024]{1,0:T(8,128)}) %reduce-scatter.11.cloned.1.call-update) | async-done | bytes 131088 | tf_op jit(solution)/shard_map/reduce_scatter | solution.py:105
  296.7 1.5 fusion.93
  (94 shorter events, 3.8 us)
Async XLA Ops:
  7.2 21.5 %copy-start.17 = (f32[2,16]{1,0:T(2,128)S(1)}, f32[2,16]{1,0:T(2,128)}, u32[]{:S(2)}) copy-start(f32[2,16]{1,0:T(2,128)} %param.21) | copy-start | bytes 388
  7.2 67.7 %reduce-scatter.5.cloned.1.call-start = ((), (), s32[]{:S(2)}) async-start(), calls=%async_computation.4 | async-start | bytes 327680 | tf_op jit(solution)/shard_map/reduce_scatter | solution.py:86
  7.2 8.2 %collective-permute-start = (bf16[32,512]{1,0:T(8,128)(2,1)}, bf16[32,512]{1,0:T(8,128)(2,1)S(1)}, u32[]{:S(2)}, u32[]{:S(2)}) collective-permute-start(bf16[32,512]{1,0:T(8,128)(2,1)} %param.16), channel_id=1, source_target_pairs={{0,4},{4,8},{8,12},{12,16},{16,20},{20,24},{24,28},{28,0},{1,5},{5... | collective-permute-start | bytes 98312 | tf_op jit(solution)/shard_map/ppermute | solution.py:75
  15.4 6.6 %collective-permute-start.1 = (bf16[32,512]{1,0:T(8,128)(2,1)S(1)}, bf16[32,512]{1,0:T(8,128)(2,1)S(1)}, u32[]{:S(2)}, u32[]{:S(2)}) collective-permute-start(bf16[32,512]{1,0:T(8,128)(2,1)S(1)} %collective-permute-done), channel_id=1, source_target_pairs={{0,4},{4,8},{8,12},{12,16},{16,20},{20,24},{24,28},{28,0},{1,5},{5... | collective-permute-start | bytes 98312 | tf_op jit(solution)/shard_map/ppermute | solution.py:75
  22.0 6.6 %collective-permute-start.2 = (bf16[32,512]{1,0:T(8,128)(2,1)S(1)}, bf16[32,512]{1,0:T(8,128)(2,1)S(1)}, u32[]{:S(2)}, u32[]{:S(2)}) collective-permute-start(bf16[32,512]{1,0:T(8,128)(2,1)S(1)} %collective-permute-done.1), channel_id=1, source_target_pairs={{0,4},{4,8},{8,12},{12,16},{16,20},{20,24},{24,28},{28,0},{1,5},{5... | collective-permute-start | bytes 98312 | tf_op jit(solution)/shard_map/ppermute | solution.py:75
  22.0 13.2 %copy-start.13 = (f32[2,16,64]{2,1,0:T(8,128)S(1)}, f32[2,16,64]{2,1,0:T(8,128)}, u32[]{:S(2)}) copy-start(f32[2,16,64]{2,1,0:T(8,128)} %param.20) | copy-start | bytes 24580
  22.0 13.2 %copy-start.14 = (f32[2,16,64]{2,1,0:T(8,128)S(1)}, f32[2,16,64]{2,1,0:T(8,128)}, u32[]{:S(2)}) copy-start(f32[2,16,64]{2,1,0:T(8,128)} %param.19) | copy-start | bytes 24580
  22.0 34.2 %copy-start.18 = (bf16[2,512,256]{2,1,0:T(8,128)(2,1)S(1)}, bf16[2,512,256]{2,1,0:T(8,128)(2,1)}, u32[]{:S(2)}) copy-start(bf16[2,512,256]{2,1,0:T(8,128)(2,1)} %param.18) | copy-start | bytes 1572868
  28.6 6.6 %collective-permute-start.3 = (bf16[32,512]{1,0:T(8,128)(2,1)S(1)}, bf16[32,512]{1,0:T(8,128)(2,1)S(1)}, u32[]{:S(2)}, u32[]{:S(2)}) collective-permute-start(bf16[32,512]{1,0:T(8,128)(2,1)S(1)} %collective-permute-done.2), channel_id=1, source_target_pairs={{0,4},{4,8},{8,12},{12,16},{16,20},{20,24},{24,28},{28,0},{1,5},{5... | collective-permute-start | bytes 98312 | tf_op jit(solution)/shard_map/ppermute | solution.py:75
  35.2 7.0 %collective-permute-start.4 = (bf16[32,512]{1,0:T(8,128)(2,1)S(1)}, bf16[32,512]{1,0:T(8,128)(2,1)S(1)}, u32[]{:S(2)}, u32[]{:S(2)}) collective-permute-start(bf16[32,512]{1,0:T(8,128)(2,1)S(1)} %collective-permute-done.3), channel_id=1, source_target_pairs={{0,4},{4,8},{8,12},{12,16},{16,20},{20,24},{24,28},{28,0},{1,5},{5... | collective-permute-start | bytes 98312 | tf_op jit(solution)/shard_map/ppermute | solution.py:75
  35.4 13.4 %copy-start.15 = (f32[2,512]{1,0:T(2,128)S(1)}, f32[2,512]{1,0:T(2,128)}, u32[]{:S(2)}) copy-start(f32[2,512]{1,0:T(2,128)} %param.17) | copy-start | bytes 12292
  42.2 6.6 %collective-permute-start.5 = (bf16[32,512]{1,0:T(8,128)(2,1)S(1)}, bf16[32,512]{1,0:T(8,128)(2,1)S(1)}, u32[]{:S(2)}, u32[]{:S(2)}) collective-permute-start(bf16[32,512]{1,0:T(8,128)(2,1)S(1)} %collective-permute-done.4), channel_id=1, source_target_pairs={{0,4},{4,8},{8,12},{12,16},{16,20},{20,24},{24,28},{28,0},{1,5},{5... | collective-permute-start | bytes 98312 | tf_op jit(solution)/shard_map/ppermute | solution.py:75
  48.8 6.6 %collective-permute-start.6 = (bf16[32,512]{1,0:T(8,128)(2,1)S(1)}, bf16[32,512]{1,0:T(8,128)(2,1)S(1)}, u32[]{:S(2)}, u32[]{:S(2)}) collective-permute-start(bf16[32,512]{1,0:T(8,128)(2,1)S(1)} %collective-permute-done.5), channel_id=1, source_target_pairs={{0,4},{4,8},{8,12},{12,16},{16,20},{20,24},{24,28},{28,0},{1,5},{5... | collective-permute-start | bytes 98312 | tf_op jit(solution)/shard_map/ppermute | solution.py:75
  55.5 0.8 copy-start.12
  57.3 0.7 copy-start.16
  57.4 95.0 %reduce-scatter.7.cloned.1.call-start = ((), (), s32[]{:S(2)}) async-start(), calls=%async_computation.5 | async-start | bytes 1179648 | tf_op jit(solution)/shard_map/reduce_scatter | solution.py:105
  58.0 0.7 copy-start.19
  60.2 15.6 %copy-start = (f32[2,16,64,16]{2,3,1,0:T(8,128)S(1)}, f32[2,16,64,16]{2,3,1,0:T(8,128)}, u32[]{:S(2)}) copy-start(f32[2,16,64,16]{2,3,1,0:T(8,128)} %param.23) | copy-start | bytes 393220
  60.2 15.6 %copy-start.1 = (f32[2,16,64,16]{2,3,1,0:T(8,128)S(1)}, f32[2,16,64,16]{2,3,1,0:T(8,128)}, u32[]{:S(2)}) copy-start(f32[2,16,64,16]{2,3,1,0:T(8,128)} %param.22) | copy-start | bytes 393220
  76.9 1.1 copy-start.10
  78.0 1.0 copy-start.6
  78.9 7.5 %copy-start.2 = (bf16[2,256,512]{2,1,0:T(8,128)(2,1)S(1)}, bf16[2,256,512]{2,1,0:T(8,128)(2,1)}, u32[]{:S(2)}) copy-start(bf16[2,256,512]{2,1,0:T(8,128)(2,1)} %param.28) | copy-start | bytes 1572868
  79.9 0.9 copy-start.8
  80.8 5.8 %copy-start.4 = (bf16[2,256,512]{2,1,0:T(8,128)(2,1)S(1)}, bf16[2,256,512]{2,1,0:T(8,128)(2,1)}, u32[]{:S(2)}) copy-start(bf16[2,256,512]{2,1,0:T(8,128)(2,1)} %param.27) | copy-start | bytes 1572868
  87.9 131.3 %reduce-scatter.9.cloned.1.call-start = ((), (), s32[]{:S(2)}) async-start(), calls=%async_computation.6 | async-start | bytes 327680 | tf_op jit(solution)/shard_map/reduce_scatter | solution.py:86
  153.3 6.7 %collective-permute-start.7 = (bf16[32,512]{1,0:T(8,128)(2,1)S(1)}, bf16[32,512]{1,0:T(8,128)(2,1)S(1)}, u32[]{:S(2)}, u32[]{:S(2)}) collective-permute-start(bf16[32,512]{1,0:T(8,128)(2,1)S(1)} %fusion.92), channel_id=1, source_target_pairs={{0,4},{4,8},{8,12},{12,16},{16,20},{20,24},{24,28},{28,0},{1,5},{5... | collective-permute-start | bytes 98312 | tf_op jit(solution)/shard_map/ppermute | solution.py:75
  159.9 6.6 %collective-permute-start.8 = (bf16[32,512]{1,0:T(8,128)(2,1)S(1)}, bf16[32,512]{1,0:T(8,128)(2,1)S(1)}, u32[]{:S(2)}, u32[]{:S(2)}) collective-permute-start(bf16[32,512]{1,0:T(8,128)(2,1)S(1)} %collective-permute-done.7), channel_id=1, source_target_pairs={{0,4},{4,8},{8,12},{12,16},{16,20},{20,24},{24,28},{28,0},{1,5},{5... | collective-permute-start | bytes 98312 | tf_op jit(solution)/shard_map/ppermute | solution.py:75
  166.5 6.7 %collective-permute-start.9 = (bf16[32,512]{1,0:T(8,128)(2,1)S(1)}, bf16[32,512]{1,0:T(8,128)(2,1)S(1)}, u32[]{:S(2)}, u32[]{:S(2)}) collective-permute-start(bf16[32,512]{1,0:T(8,128)(2,1)S(1)} %collective-permute-done.8), channel_id=1, source_target_pairs={{0,4},{4,8},{8,12},{12,16},{16,20},{20,24},{24,28},{28,0},{1,5},{5... | collective-permute-start | bytes 98312 | tf_op jit(solution)/shard_map/ppermute | solution.py:75
  173.3 6.6 %collective-permute-start.10 = (bf16[32,512]{1,0:T(8,128)(2,1)S(1)}, bf16[32,512]{1,0:T(8,128)(2,1)S(1)}, u32[]{:S(2)}, u32[]{:S(2)}) collective-permute-start(bf16[32,512]{1,0:T(8,128)(2,1)S(1)} %collective-permute-done.9), channel_id=1, source_target_pairs={{0,4},{4,8},{8,12},{12,16},{16,20},{20,24},{24,28},{28,0},{1,5},{5... | collective-permute-start | bytes 98312 | tf_op jit(solution)/shard_map/ppermute | solution.py:75
  179.9 6.6 %collective-permute-start.11 = (bf16[32,512]{1,0:T(8,128)(2,1)S(1)}, bf16[32,512]{1,0:T(8,128)(2,1)S(1)}, u32[]{:S(2)}, u32[]{:S(2)}) collective-permute-start(bf16[32,512]{1,0:T(8,128)(2,1)S(1)} %collective-permute-done.10), channel_id=1, source_target_pairs={{0,4},{4,8},{8,12},{12,16},{16,20},{20,24},{24,28},{28,0},{1,5},{5... | collective-permute-start | bytes 98312 | tf_op jit(solution)/shard_map/ppermute | solution.py:75
  186.5 6.6 %collective-permute-start.12 = (bf16[32,512]{1,0:T(8,128)(2,1)S(1)}, bf16[32,512]{1,0:T(8,128)(2,1)S(1)}, u32[]{:S(2)}, u32[]{:S(2)}) collective-permute-start(bf16[32,512]{1,0:T(8,128)(2,1)S(1)} %collective-permute-done.11), channel_id=1, source_target_pairs={{0,4},{4,8},{8,12},{12,16},{16,20},{20,24},{24,28},{28,0},{1,5},{5... | collective-permute-start | bytes 98312 | tf_op jit(solution)/shard_map/ppermute | solution.py:75
  193.1 6.6 %collective-permute-start.13 = (bf16[32,512]{1,0:T(8,128)(2,1)S(1)}, bf16[32,512]{1,0:T(8,128)(2,1)S(1)}, u32[]{:S(2)}, u32[]{:S(2)}) collective-permute-start(bf16[32,512]{1,0:T(8,128)(2,1)S(1)} %collective-permute-done.12), channel_id=1, source_target_pairs={{0,4},{4,8},{8,12},{12,16},{16,20},{20,24},{24,28},{28,0},{1,5},{5... | collective-permute-start | bytes 98312 | tf_op jit(solution)/shard_map/ppermute | solution.py:75
  201.8 94.9 %reduce-scatter.11.cloned.1.call-start = ((), (), s32[]{:S(2)}) async-start(), calls=%async_computation.7 | async-start | bytes 1179648 | tf_op jit(solution)/shard_map/reduce_scatter | solution.py:105
  221.3 1.1 copy-start.11
  222.4 1.0 copy-start.7
  223.3 7.4 %copy-start.3 = (bf16[2,256,512]{2,1,0:T(8,128)(2,1)S(1)}, bf16[2,256,512]{2,1,0:T(8,128)(2,1)}, u32[]{:S(2)}) copy-start(bf16[2,256,512]{2,1,0:T(8,128)(2,1)} %param.28) | copy-start | bytes 1572868
  224.3 0.9 copy-start.9
  225.2 5.8 %copy-start.5 = (bf16[2,256,512]{2,1,0:T(8,128)(2,1)S(1)}, bf16[2,256,512]{2,1,0:T(8,128)(2,1)}, u32[]{:S(2)}) copy-start(bf16[2,256,512]{2,1,0:T(8,128)(2,1)} %param.27) | copy-start | bytes 1572868
Sparse Core Ops, SparseCore 0:
  57.5 17.3 reduce-scatter.4
  88.1 64.2 reduce-scatter.6
  202.0 17.2 reduce-scatter.8
  232.5 64.1 reduce-scatter.10
